TPU v7x, 32 devices: a whole 2x2x4 slice. The times are simulated.
32 devices in a mesh: ep: 8 (over z, core), tp: 4 (over y, x).
Axes of the slice: x: 2, y: 2, z: 4, core: 2. Of those that a mesh axis runs over, the one named last changes fastest.
Arguments:
- receptance: bfloat16 [2048, 2048], P('ep', 'tp'), may hold values from -6 to 6
- key_tensor: bfloat16 [2048, 2048], P('ep', 'tp'), may hold values from -6 to 6
- value_tensor: bfloat16 [2048, 2048], P('ep', 'tp'), may hold values from -6 to 6
- decay_data_input: bfloat16 [2048, 2048], P('ep', 'tp'), may hold values from -4 to 4
- correction_rate_input: bfloat16 [2048, 2048], P('ep', 'tp'), may hold values from -16 to 6
- mixer_output_gate: bfloat16 [2048, 2048], P('ep', 'tp'), may hold values from -6 to 6
- decay_channel_offset: float32 [2048], P('tp'), may hold values from -16 to -3
- head_norm_gain: float32 [2048], P('tp'), may hold values from 0.1 to 1.9
- self_key_weight: float32 [2048], P('tp'), may hold values from -2 to 2
- mixer_output_weight: bfloat16 [2048, 2048], P('tp'), may hold values from -0.125 to 0.125
- second_batch_rows: bfloat16 [1024, 2048], P('ep'), may hold values from -6 to 6
- routed_expert_index: int32 [1024, 4], P('ep'), may hold values from 0 to 7, all different within a row; in each aligned block of 128 rows (0 to 127, 128 to 255, ...) at most 96 rows name the same one
- routing_output_weight: float32 [1024, 4], P('ep'), may hold values from 0.1 to 1
- expert_norm_gain: float32 [2048], replicated, may hold values from 0.1 to 1.9
- expert_gate_weight: bfloat16 [8, 1024, 2048], P('ep', 'tp'), may hold values from -0.125 to 0.125
- expert_up_weight: bfloat16 [8, 1024, 2048], P('ep', 'tp'), may hold values from -0.125 to 0.125
- expert_down_weight: bfloat16 [8, 1024, 2048], P('ep', None, 'tp'), may hold values from -0.1875 to 0.1875
- common_expert_gate: bfloat16 [1024, 2048], P('tp'), may hold values from -0.125 to 0.125
- common_expert_up: bfloat16 [1024, 2048], P('tp'), may hold values from -0.125 to 0.125
- common_expert_down: bfloat16 [1024, 2048], P(None, 'tp'), may hold values from -0.1875 to 0.1875
Outputs:
- token_mixer_output: bfloat16 [2048, 2048], P(('ep', 'tp'))
- expert_out: bfloat16 [1024, 2048], P('ep', 'tp')
Inputs may be any that keep to these rules, and one draw needn't show every extreme that they name: `routed_expert_index`: each row names 4 different experts. Within the rows of one index of ep no expert is named by more than 96 rows, and that bound is met in some index's rows.
All inputs are finite; a program needn't handle non-finite values.
Results may differ from a plain program's by a relative error of at most 0.017.
Values may be sent and summed in bfloat16 or wider, within the bound.
A program may use at most 128 MiB of HBM per device.

v0:
```python
import math
import jax
import jax.numpy as jnp
from jax import lax
from jax.sharding import PartitionSpec as P

HEAD_CHANNELS = 64
SPAN = 64
HIGHEST = lax.Precision.HIGHEST
PRECISION = lax.Precision.HIGH
NORM_FLOOR = 1.0


def head_view(matrix):
    return matrix.astype(jnp.float32).reshape(matrix.shape[0], -1, HEAD_CHANNELS)


def complete_head_outputs(
    state_readout,
    receptance_rows,
    key_row_block,
    value_row_block,
    head_norm_gain,
    self_key_weight,
    mixer_output_gate,
):
    mean_part = jnp.mean(state_readout, axis=-1, keepdims=True)
    spread = jnp.mean(jnp.square(state_readout - mean_part), axis=-1, keepdims=True)
    normalized_rows = (state_readout - mean_part) * lax.rsqrt(spread + NORM_FLOOR)
    sequence_length = state_readout.shape[0]
    normalized_rows = normalized_rows.reshape(sequence_length, -1) * head_norm_gain
    self_key_term = (
        jnp.sum(
            receptance_rows * key_row_block * self_key_weight.reshape(-1, HEAD_CHANNELS),
            axis=-1,
            keepdims=True,
        )
        * value_row_block
    )
    mixer_result = (
        normalized_rows + self_key_term.reshape(sequence_length, -1)
    ) * mixer_output_gate.astype(jnp.float32)
    return mixer_result.astype(jnp.bfloat16)


def product(spec, left, right):
    return jnp.einsum(spec, left, right, precision=PRECISION, preferred_element_type=jnp.float32)


def lower_inverse(strict, size):
    at = jnp.arange(size)
    row, column = (at[:, None], at[None, :])
    inverse = None
    block = 1
    while block < size:
        pair = (
            (row // (2 * block) == column // (2 * block))
            & (row // block % 2 == 1)
            & (column // block % 2 == 0)
        )
        below = jnp.where(pair, strict, 0.0)
        if inverse is None:
            inverse = jnp.eye(size, dtype=jnp.float32) - below
        else:
            inverse = inverse - product(
                "nhij,nhjk->nhik", product("nhij,nhjk->nhik", inverse, below), inverse
            )
        block *= 2
    return inverse


def mixer_part(
    receptance,
    key_tensor,
    value_tensor,
    decay_data_input,
    correction_rate_input,
    mixer_output_gate,
    decay_channel_offset,
    head_norm_gain,
    self_key_weight,
    mixer_output_weight,
    routed_pieces,
):
    row_count, width = receptance.shape
    head_count = width // HEAD_CHANNELS
    span = min(SPAN, row_count)
    block_count = row_count // span
    receptance_rows = head_view(receptance)
    key_row_block = head_view(key_tensor)
    value_row_block = head_view(value_tensor)

    def by_block(matrix):
        return (
            matrix.astype(jnp.float32)
            .reshape(block_count, span, head_count, HEAD_CHANNELS)
            .transpose(0, 2, 1, 3)
        )

    step_log = -math.exp(-0.5) * jax.nn.sigmoid(
        decay_channel_offset + decay_data_input.astype(jnp.float32)
    )
    at = jnp.arange(span)
    reach = (at[:, None] >= at[None, :]).astype(jnp.float32)
    step_log = by_block(step_log)
    total_log = jnp.einsum("ts,nhsd->nhtd", reach, step_log, precision=HIGHEST)
    recept, keys, values = (by_block(receptance), by_block(key_tensor), by_block(value_tensor))
    units = keys * lax.rsqrt(jnp.sum(keys * keys, axis=-1, keepdims=True) + 1.0)
    corrections = units * jax.nn.sigmoid(by_block(correction_rate_input))
    grown = jnp.exp(-total_log)
    last_log = total_log[:, :, -1:, :]
    unit_in = units * jnp.exp(total_log - step_log)
    recept_in = recept * jnp.exp(total_log)
    tail = jnp.exp(last_log - total_log)
    scores = product(
        "nhtd,nhsd->nhts",
        jnp.concatenate([unit_in, recept_in], axis=2),
        jnp.concatenate([keys * grown, corrections * grown], axis=2),
    )
    before = at[:, None] > at[None, :]
    upto = at[:, None] >= at[None, :]
    unit_key = jnp.where(before, scores[:, :, :span, :span], 0.0)
    unit_fix = jnp.where(before, scores[:, :, :span, span:], 0.0)
    read_key = jnp.where(upto, scores[:, :, span:, :span], 0.0)
    read_fix = jnp.where(upto, scores[:, :, span:, span:], 0.0)
    inverse = lower_inverse(unit_fix, span)
    key_values = product("nhts,nhsd->nhtd", jnp.concatenate([unit_key, read_key], axis=2), values)
    solved = product(
        "nhts,nhsd->nhtd", inverse, jnp.concatenate([unit_in, key_values[:, :, :span]], axis=3)
    )
    reads = jnp.concatenate([recept_in, key_values[:, :, span:]], axis=3) - product(
        "nhts,nhsd->nhtd", read_fix, solved
    )
    eye_head = jnp.eye(HEAD_CHANNELS, dtype=jnp.float32)
    fresh = product("nhtj,nhti->nhji", keys * tail, values)
    moves = jnp.concatenate([eye_head * jnp.exp(last_log), fresh], axis=3) - product(
        "nhtj,nhti->nhji", corrections * tail, solved
    )
    whole = moves[0]
    for block in range(1, block_count):
        step = product("hij,hjk->hik", moves[block, :, :, :HEAD_CHANNELS], whole)
        whole = step + jnp.concatenate(
            [jnp.zeros_like(step[..., :HEAD_CHANNELS]), moves[block, :, :, HEAD_CHANNELS:]], axis=2
        )
    whole, routed_pieces = lax.optimization_barrier((whole, routed_pieces))
    everything = lax.all_gather(whole.astype(jnp.bfloat16), "ep")
    mine = lax.axis_index("ep")
    state = jnp.zeros((head_count, HEAD_CHANNELS, HEAD_CHANNELS), jnp.float32)
    for k in range(lax.axis_size("ep") - 1):
        part = everything[k].astype(jnp.float32)
        new = product("hij,hjk->hik", part[..., :HEAD_CHANNELS], state)
        state = jnp.where(k < mine, new + part[..., HEAD_CHANNELS:], state)
    starts = [state]
    for block in range(block_count - 1):
        state = (
            product("hij,hjk->hik", moves[block, :, :, :HEAD_CHANNELS], state)
            + moves[block, :, :, HEAD_CHANNELS:]
        )
        starts.append(state)
    merged_output = reads[..., HEAD_CHANNELS:] + product(
        "nhtj,nhji->nhti", reads[..., :HEAD_CHANNELS], jnp.stack(starts)
    )
    merged_output = merged_output.transpose(0, 2, 1, 3).reshape(
        row_count, head_count, HEAD_CHANNELS
    )
    mixer_result = complete_head_outputs(
        merged_output,
        receptance_rows,
        key_row_block,
        value_row_block,
        head_norm_gain,
        self_key_weight,
        mixer_output_gate,
    )
    summed = lax.psum_scatter(
        jnp.dot(mixer_result, mixer_output_weight, preferred_element_type=jnp.float32).astype(
            jnp.bfloat16
        ),
        "tp",
        scatter_dimension=0,
        tiled=True,
    )
    return (summed, routed_pieces)


def activate(rows_in, gate_part, up_part):
    pre_gate = jnp.einsum("fd,rd->fr", gate_part, rows_in, preferred_element_type=jnp.float32)
    pre_up = jnp.einsum("fd,rd->fr", up_part, rows_in, preferred_element_type=jnp.float32)
    return (jax.nn.silu(pre_gate) * pre_up).astype(jnp.bfloat16)


def expert_entry(
    second_batch_rows,
    routed_expert_index,
    routing_output_weight,
    expert_norm_gain,
    common_expert_gate,
    common_expert_up,
):
    row_count, width = second_batch_rows.shape
    top_count = routed_expert_index.shape[1]
    peer_count = lax.axis_size("ep")
    slot_count = 3 * row_count * top_count // (2 * peer_count)
    widened = second_batch_rows.astype(jnp.float32)
    normalized_rows = (
        widened
        * lax.rsqrt(jnp.mean(widened * widened, axis=-1, keepdims=True) + NORM_FLOOR)
        * expert_norm_gain
    ).astype(jnp.bfloat16)
    flat_ids = routed_expert_index.reshape(-1)
    one_hot = (flat_ids[:, None] == jnp.arange(peer_count, dtype=jnp.int32)[None, :]).astype(
        jnp.int32
    )
    slot_rank = jnp.sum((jnp.cumsum(one_hot, axis=0) - 1) * one_hot, axis=1)
    target = flat_ids * slot_count + slot_rank
    owners = jnp.arange(row_count * top_count, dtype=jnp.int32) // top_count
    source_row = jnp.full((peer_count * slot_count,), row_count, jnp.int32).at[target].set(owners)
    padded = jnp.concatenate([normalized_rows, jnp.zeros((1, width), jnp.bfloat16)], axis=0)
    outgoing = jnp.take(padded, source_row, axis=0).reshape(peer_count, slot_count, width)
    shared_hidden = activate(normalized_rows, common_expert_gate, common_expert_up)
    piece_width = width // lax.axis_size("tp")
    own_slice = lax.dynamic_slice_in_dim(
        outgoing, lax.axis_index("tp") * piece_width, piece_width, 2
    )
    arrived = lax.all_to_all(own_slice, "ep", split_axis=0, concat_axis=0, tiled=True)
    return (arrived, shared_hidden, target)


def expert_exit(
    slots,
    pieces,
    shared_hidden,
    target,
    routing_output_weight,
    expert_gate_weight,
    expert_up_weight,
    expert_down_weight,
    common_expert_down,
):
    peer_count, slot_count = slots
    row_count, top_count = routing_output_weight.shape
    out_width = expert_down_weight.shape[2]
    gate_cols = expert_gate_weight[0]
    up_cols = expert_up_weight[0]
    pre_gate = jnp.einsum("fd,rd->fr", gate_cols, pieces, preferred_element_type=jnp.float32)
    pre_up = jnp.einsum("fd,rd->fr", up_cols, pieces, preferred_element_type=jnp.float32)
    routed_hidden = (jax.nn.silu(pre_gate) * pre_up).astype(jnp.bfloat16)
    both = lax.all_gather(
        jnp.concatenate([routed_hidden, shared_hidden], axis=1), "tp", axis=0, tiled=True
    )
    pieces = (both[:, : routed_hidden.shape[1]], both[:, routed_hidden.shape[1] :])
    routed_rows = expert_down_weight[0]
    routed_sum = jnp.einsum("fr,fd->rd", pieces[0], routed_rows, preferred_element_type=jnp.float32)
    shared_out = jnp.einsum(
        "fr,fd->rd", pieces[1], common_expert_down, preferred_element_type=jnp.float32
    )
    returned = lax.all_to_all(
        routed_sum.astype(jnp.bfloat16).reshape(peer_count, slot_count, out_width),
        "ep",
        split_axis=0,
        concat_axis=0,
        tiled=True,
    )
    picked = jnp.take(returned.reshape(-1, out_width), target, axis=0).reshape(
        row_count, top_count, out_width
    )
    merged_output = (
        jnp.sum(picked.astype(jnp.float32) * routing_output_weight[:, :, None], axis=1) + shared_out
    )
    return merged_output.astype(jnp.bfloat16)


def on_device(
    receptance,
    key_tensor,
    value_tensor,
    decay_data_input,
    correction_rate_input,
    mixer_output_gate,
    decay_channel_offset,
    head_norm_gain,
    self_key_weight,
    mixer_output_weight,
    second_batch_rows,
    routed_expert_index,
    routing_output_weight,
    expert_norm_gain,
    expert_gate_weight,
    expert_up_weight,
    expert_down_weight,
    common_expert_gate,
    common_expert_up,
    common_expert_down,
):
    arrived, shared_hidden, target = expert_entry(
        second_batch_rows,
        routed_expert_index,
        routing_output_weight,
        expert_norm_gain,
        common_expert_gate,
        common_expert_up,
    )
    arrived, receptance, key_tensor, value_tensor, decay_data_input, correction_rate_input = (
        lax.optimization_barrier(
            (arrived, receptance, key_tensor, value_tensor, decay_data_input, correction_rate_input)
        )
    )
    flat_rows = arrived.reshape(-1, arrived.shape[2])
    pieces = lax.all_gather(flat_rows, "tp", axis=1, tiled=True)
    token_mixer_output, pieces = mixer_part(
        receptance,
        key_tensor,
        value_tensor,
        decay_data_input,
        correction_rate_input,
        mixer_output_gate,
        decay_channel_offset,
        head_norm_gain,
        self_key_weight,
        mixer_output_weight,
        pieces,
    )
    expert_out = expert_exit(
        arrived.shape[:2],
        pieces,
        shared_hidden,
        target,
        routing_output_weight,
        expert_gate_weight,
        expert_up_weight,
        expert_down_weight,
        common_expert_down,
    )
    return (token_mixer_output, expert_out)


def solution(mesh):
    in_specs = (
        P("ep", "tp"),
        P("ep", "tp"),
        P("ep", "tp"),
        P("ep", "tp"),
        P("ep", "tp"),
        P("ep", "tp"),
        P("tp"),
        P("tp"),
        P("tp"),
        P("tp", None),
        P("ep", None),
        P("ep", None),
        P("ep", None),
        P(),
        P("ep", "tp", None),
        P("ep", "tp", None),
        P("ep", None, "tp"),
        P("tp", None),
        P("tp", None),
        P(None, "tp"),
    )
    out_specs = (P(("ep", "tp"), None), P("ep", "tp"))
    return jax.shard_map(
        on_device, mesh=mesh, in_specs=in_specs, out_specs=out_specs, check_vma=False
    )
```

profile of v0, /device:TPU:0, one launch (start us, length us, event | category | flops | bytes accessed | tf_op | source)
XLA Modules:
  0.0 222.1 jit_solution(11237634688748817533)
XLA Ops:
  10.8 2.4 %scatter_custom_fusion = s32[768]{0:T(1024)S(1)} fusion(s32[512]{0:T(512)S(1)} %bitcast.191, s32[512]{0:T(512)S(1)} %add_select_fusion, s32[]{:T(128)} %constant.328.clone.1), kind=kCustom, calls=%fused_computation.207 | custom fusion | bytes 3076 | tf_op jit(solution)/shard_map/scatter | solution.py:217
  15.9 4.3 %gather_fusion = bf16[768,2048]{1,0:T(8,128)(2,1)} fusion(bf16[129,2048]{1,0:T(8,128)(2,1)S(1)} %concatenate.33, s32[1024]{0:T(1024)S(1)} %pad_clamp_fusion.1), kind=kCustom, calls=%fused_computation | custom fusion | bytes 6294528 | tf_op jit(solution)/shard_map/jit(_take)/gather | solution.py:219
  20.2 2.3 %dynamic-slice_select_fusion = bf16[8,96,512]{2,1,0:T(8,128)(2,1)} fusion(bf16[8,96,2048]{2,1,0:T(8,128)(2,1)} %bitcast.177, s32[]{:T(128)S(6)} %select_n.364, pred[8,96]{1,0:T(8,128)(4,1)S(1)} %broadcast_in_dim.94), kind=kLoop, calls=%fused_computation.114 | loop fusion | flops 393216 | bytes 1573636 | tf_op jit(solution)/shard_map/jit(_take)/select_n | solution.py:219
  22.4 6.5 %all-to-all-start = ((bf16[8,96,512]{2,1,0:T(8,128)(2,1)}), bf16[8,96,512]{2,1,0:T(8,128)(2,1)}, u32[]{:S(2)}, u32[]{:S(2)}) async-start(bf16[8,96,512]{2,1,0:T(8,128)(2,1)} %dynamic-slice_select_fusion), calls=%async_computation | async-start | bytes 1572864 | tf_op jit(solution)/shard_map/all_to_all | solution.py:225
  29.9 2.4 %convolution_bitcast_fusion.4 = f32[256,128]{0,1:T(8,128)} fusion(bf16[128,2048]{1,0:T(8,128)(2,1)S(1)} %fusion.33, bf16[256,2048]{1,0:T(8,128)(2,1)} %param.37), kind=kOutput, calls=%fused_computation.60 | convolution fusion | flops 134217728 | bytes 1703936 | tf_op jit(solution)/shard_map/fd,rd->fr/dot_general | solution.py:187
  32.3 17.7 %all-to-all-done = bf16[8,96,512]{2,1,0:T(8,128)(2,1)} async-done(((bf16[8,96,512]{2,1,0:T(8,128)(2,1)}), bf16[8,96,512]{2,1,0:T(8,128)(2,1)}, u32[]{:S(2)}, u32[]{:S(2)}) %all-to-all-start) | async-done | bytes 786464 | tf_op jit(solution)/shard_map/all_to_all | solution.py:225
  51.0 2.1 add_divide_fusion
  57.7 2.3 %reshape.834 = f32[4,64,8,64]{3,2,1,0:T(8,128)} reshape(f32[256,512]{1,0:T(8,128)} %get-tuple-element.35) | data formatting | bytes 1048576 | tf_op jit(solution)/shard_map/reshape | solution.py:96
  59.9 2.4 %reshape.884 = f32[4,64,8,64]{1,0,3,2:T(4,128)} reshape(bf16[256,512]{0,1:T(8,128)(2,1)} %copy.246) | data formatting | bytes 786432 | tf_op jit(solution)/shard_map/reshape | solution.py:96
  62.3 2.6 %copy.248 = f32[4,64,8,64]{3,1,2,0:T(8,128)} copy(f32[4,64,8,64]{1,0,3,2:T(4,128)} %reshape.884) | data formatting | bytes 1048576 | tf_op jit(solution)/shard_map/reshape | solution.py:96
  64.8 5.0 %fusion.66 = (f32[4,8,64,64]{3,2,1,0:T(8,128)S(1)}, f32[4,8,64,64]{3,2,1,0:T(8,128)S(1)}, f32[4,8,64,64]{3,2,1,0:T(8,128)S(1)}, f32[4,8,64,64]{3,2,1,0:T(8,128)S(1)}, f32[4,8,64,64]{3,2,1,0:T(8,128)}) fusion(f32[4,64,8,64]{3,2,1,0:T(8,128)} %reshape.842, f32[4,8,64]{2,1,0:T(8,128)S(1)} %add_rsqrt_fusion.1, f32[4,64,8,64]{3,1,2,0:T(8,128)S(1)} %copy.252, ...), kind=kOutput, calls=%fused_computation.113 | convolution fusion | flops 101715968 | bytes 4726784 | tf_op jit(solution)/shard_map/ts,nhsd->nhtd/dot_general | solution.py:106
  69.8 2.3 %fusion.1 = f32[4,8,128,128]{3,2,1,0:T(8,128)S(1)} fusion(f32[4,8,64,64]{3,2,1,0:T(8,128)S(1)} %get-tuple-element.30, f32[4,8,64,64]{3,2,1,0:T(8,128)S(1)} %get-tuple-element.19, f32[4,8,64,64]{3,2,1,0:T(8,128)S(1)} %get-tuple-element.18, f32[4,8,64,64]{3,2,1,0:T(8,128)S(1)} %get-tuple-element.24), kind=kOutput, calls=%fused_computation.5 | convolution fusion | flops 201850880 | bytes 4194304 | tf_op jit(solution)/shard_map/nhtd,nhsd->nhts/dot_general | solution.py:47
  79.9 2.6 %fusion.8 = f32[4,8,128,64]{3,2,1,0:T(8,128)S(1)} fusion(f32[4,8,64,64]{3,2,1,0:T(8,128)} %get-tuple-element.23, f32[4,8,64,64]{3,2,1,0:T(8,128)} %get-tuple-element.22, bf16[4,8,64,64]{3,1,2,0:T(8,128)(2,1)} %bitcast.178), kind=kOutput, calls=%fused_computation.12 | convolution fusion | flops 100925440 | bytes 2359296 | tf_op jit(solution)/shard_map/nhts,nhsd->nhtd/dot_general | solution.py:47
  96.7 25.7 %all-gather.5.cloned.1.call-done = bf16[768,2048]{1,0:T(8,128)(2,1)} async-done(((bf16[768,512]{1,0:T(8,128)(2,1)}), bf16[768,2048]{1,0:T(8,128)(2,1)}) %all-gather.5.cloned.1.call-update) | async-done | bytes 3145744 | tf_op jit(solution)/shard_map/all_gather | solution.py:309
  122.8 2.5 %fusion.30 = bf16[256,128]{0,1:T(8,128)(2,1)} fusion(bf16[128,2048]{1,0:T(8,128)(2,1)} %copy-done.14, bf16[256,2048]{1,0:T(8,128)(2,1)} %param.38, f32[256,128]{0,1:T(8,128)S(1)} %copy-done.19), kind=kOutput, calls=%fused_computation.61 | convolution fusion | flops 134414336 | bytes 1769472 | tf_op jit(solution)/shard_map/fd,rd->fr/dot_general | solution.py:188
  130.1 3.9 %convolution_subtract_fusion.6 = f32[4,8,64,128]{3,2,1,0:T(8,128)} fusion(f32[4,8,64,128]{3,2,1,0:T(8,128)} %copy-done.10, f32[4,8,128,128]{3,2,1,0:T(8,128)} %copy-done.1, f32[4,8,64,64]{3,2,1,0:T(8,128)} %get-tuple-element.20, f32[4,8,64,64]{3,2,1,0:T(8,128)S(1)} %copy-done.9, pred[64,64]{1,0:T(8,128)(4,1)S(1)} %iota_compare_fusion.2), kind=kOutput, calls=%fused_computation.27 | convolution fusion | flops 101318656 | bytes 4722688 | tf_op jit(solution)/shard_map/nhts,nhsd->nhtd/dot_general | solution.py:47
  137.1 9.7 %all-gather.9.cloned.1.call-done = bf16[64,64,128]{2,1,0:T(8,128)(2,1)} async-done(((bf16[8,64,128]{2,1,0:T(8,128)(2,1)}), bf16[64,64,128]{2,1,0:T(8,128)(2,1)}) %all-gather.9.cloned.1.call-update) | async-done | bytes 1048592 | tf_op jit(solution)/shard_map/all_gather | solution.py:146
  159.4 2.1 copy.273
  162.9 3.2 %convolution_convert_fusion = bf16[256,2048]{1,0:T(8,128)(2,1)} fusion(bf16[512,2048]{1,0:T(8,128)(2,1)S(1)} %copy-done, bf16[256,512]{1,0:T(8,128)(2,1)} %param.25, f32[256,512]{1,0:T(8,128)} %copy.274, bf16[256,512]{1,0:T(8,128)(2,1)S(1)} %copy-done.16, f32[256,512]{1,0:T(8,128)} %copy.273, f32[256,512]{1,0:T(8,128)} %reshape.838, ...), kind=kOutput, calls=%fused_computation.4 | convolution fusion | flops 538574848 | bytes 5769216 | tf_op jit(solution)/shard_map/dot_general | solution.py:176
  166.2 15.0 %all-gather.7.cloned.1.call-done = bf16[1024,896]{0,1:T(8,128)(2,1)} async-done(((bf16[256,896]{0,1:T(8,128)(2,1)}), bf16[1024,896]{0,1:T(8,128)(2,1)}) %all-gather.7.cloned.1.call-update) | async-done | bytes 1835024 | tf_op jit(solution)/shard_map/all_gather | solution.py:248
  181.2 3.6 %fusion.14 = bf16[768,512]{1,0:T(8,128)(2,1)} fusion(bf16[1024,896]{0,1:T(8,128)(2,1)} %all-gather.7.cloned.1.call-done, bf16[1,1024,512]{2,1,0:T(8,128)(2,1)} %param.36), kind=kOutput, calls=%fused_computation.23 | convolution fusion | flops 805699584 | bytes 3407872 | tf_op jit(solution)/shard_map/fr,fd->rd/dot_general | solution.py:253
  184.8 4.6 %all-to-all-start.1 = ((bf16[8,96,512]{2,1,0:T(8,128)(2,1)}), bf16[8,96,512]{2,1,0:T(8,128)(2,1)S(1)}, u32[]{:S(2)}, u32[]{:S(2)}) async-start(bf16[8,96,512]{2,1,0:T(8,128)(2,1)} %bitcast.186), calls=%async_computation.2 | async-start | bytes 1572864 | tf_op jit(solution)/shard_map/all_to_all | solution.py:257
  189.8 20.5 %all-to-all-done.1 = bf16[8,96,512]{2,1,0:T(8,128)(2,1)S(1)} async-done(((bf16[8,96,512]{2,1,0:T(8,128)(2,1)}), bf16[8,96,512]{2,1,0:T(8,128)(2,1)S(1)}, u32[]{:S(2)}, u32[]{:S(2)}) %all-to-all-start.1) | async-done | bytes 786464 | tf_op jit(solution)/shard_map/all_to_all | solution.py:257
  213.3 2.3 %fusion.28 = bf16[128,512]{1,0:T(8,128)(2,1)} fusion(f32[128,512]{1,0:T(8,128)S(1)} %multiply_reduce_fusion, bf16[1024,512]{1,0:T(8,128)(2,1)} %param.39, bf16[1024,896]{0,1:T(8,128)(2,1)} %all-gather.7.cloned.1.call-done), kind=kOutput, calls=%fused_computation.57 | convolution fusion | flops 134348800 | bytes 1703936 | tf_op jit(solution)/shard_map/fr,fd->rd/dot_general | solution.py:254
  (175 shorter events, 59.6 us)
Async XLA Ops:
  7.2 155.7 %copy-start = (bf16[512,2048]{1,0:T(8,128)(2,1)S(1)}, bf16[512,2048]{1,0:T(8,128)(2,1)}, u32[]{:S(2)}) copy-start(bf16[512,2048]{1,0:T(8,128)(2,1)} %param.29) | copy-start | bytes 6291460
  15.8 14.1 %copy-start.14 = (bf16[128,2048]{1,0:T(8,128)(2,1)}, bf16[128,2048]{1,0:T(8,128)(2,1)S(1)}, u32[]{:S(2)}) copy-start(bf16[128,2048]{1,0:T(8,128)(2,1)S(1)} %fusion.33) | copy-start | bytes 1572868
  22.4 27.5 %copy-start.17 = (bf16[256,512]{1,0:T(8,128)(2,1)S(1)}, bf16[256,512]{1,0:T(8,128)(2,1)}, u32[]{:S(2)}) copy-start(bf16[256,512]{1,0:T(8,128)(2,1)} %param.21) | copy-start | bytes 786436
  22.4 27.7 %copy-start.18 = (bf16[256,512]{1,0:T(8,128)(2,1)S(1)}, bf16[256,512]{1,0:T(8,128)(2,1)}, u32[]{:S(2)}) copy-start(bf16[256,512]{1,0:T(8,128)(2,1)} %param.20) | copy-start | bytes 786436
  22.4 28.5 %copy-start.22 = (f32[512]{0:T(512)S(1)}, f32[512]{0:T(512)}, u32[]{:S(2)}) copy-start(f32[512]{0:T(512)} %param.26) | copy-start | bytes 6148
  22.4 27.5 %all-to-all-start = ((bf16[8,96,512]{2,1,0:T(8,128)(2,1)}), bf16[8,96,512]{2,1,0:T(8,128)(2,1)}, u32[]{:S(2)}, u32[]{:S(2)}) async-start(bf16[8,96,512]{2,1,0:T(8,128)(2,1)} %dynamic-slice_select_fusion), calls=%async_computation | async-start | bytes 1572864 | tf_op jit(solution)/shard_map/all_to_all | solution.py:225
  28.9 93.5 %all-gather.5.cloned.1.call-start = ((), (), s32[]{:S(2)}) async-start(), calls=%async_computation.3 | async-start | bytes 3932160 | tf_op jit(solution)/shard_map/all_gather | solution.py:309
  72.1 2.9 %copy-start.1 = (f32[4,8,128,128]{3,2,1,0:T(8,128)}, f32[4,8,128,128]{3,2,1,0:T(8,128)S(1)}, u32[]{:S(2)}) copy-start(f32[4,8,128,128]{3,2,1,0:T(8,128)S(1)} %fusion.1) | copy-start | bytes 6291460
  79.6 67.2 %all-gather.9.cloned.1.call-start = ((), (), s32[]{:S(2)}) async-start(), calls=%async_computation.6 | async-start | bytes 1179648 | tf_op jit(solution)/shard_map/all_gather | solution.py:146
  79.9 2.8 %copy-start.2 = (f32[4,8,128,128]{3,2,1,0:T(8,128)S(1)}, f32[4,8,128,128]{3,2,1,0:T(8,128)}, u32[]{:S(2)}) copy-start(f32[4,8,128,128]{3,2,1,0:T(8,128)} %copy-done.1) | copy-start | bytes 6291460
  91.3 3.5 %copy-start.10 = (f32[4,8,64,128]{3,2,1,0:T(8,128)}, f32[4,8,64,128]{3,2,1,0:T(8,128)S(1)}, u32[]{:S(2)}) copy-start(f32[4,8,64,128]{3,2,1,0:T(8,128)S(1)} %fusion.35) | copy-start | bytes 3145732
  94.8 28.0 %copy-start.19 = (f32[256,128]{0,1:T(8,128)S(1)}, f32[256,128]{0,1:T(8,128)}, u32[]{:S(2)}) copy-start(f32[256,128]{0,1:T(8,128)} %convolution_bitcast_fusion.4) | copy-start | bytes 393220
  122.5 7.6 %copy-start.9 = (f32[4,8,64,64]{3,2,1,0:T(8,128)S(1)}, f32[4,8,64,64]{3,2,1,0:T(8,128)}, u32[]{:S(2)}) copy-start(f32[4,8,64,64]{3,2,1,0:T(8,128)} %copy-done.8) | copy-start | bytes 1572868
  122.5 58.7 %all-gather.7.cloned.1.call-start = ((), (), s32[]{:S(2)}) async-start(), calls=%async_computation.5 | async-start | bytes 2293760 | tf_op jit(solution)/shard_map/all_gather | solution.py:248
  130.0 3.9 %copy-start.25 = (bf16[768,2048]{1,0:T(8,128)(2,1)S(1)}, bf16[768,2048]{1,0:T(8,128)(2,1)}, u32[]{:S(2)}) copy-start(bf16[768,2048]{1,0:T(8,128)(2,1)} %all-gather.5.cloned.1.call-done) | copy-start | bytes 9437188
  130.0 3.9 %copy-start.26 = (bf16[1,256,2048]{2,1,0:T(8,128)(2,1)S(1)}, bf16[1,256,2048]{2,1,0:T(8,128)(2,1)}, u32[]{:S(2)}) copy-start(bf16[1,256,2048]{2,1,0:T(8,128)(2,1)} %param.34) | copy-start | bytes 3145732
  137.1 18.3 %copy-start.4 = (f32[4,8,64,128]{3,2,1,0:T(8,128)S(1)}, f32[4,8,64,128]{3,2,1,0:T(8,128)}, u32[]{:S(2)}) copy-start(f32[4,8,64,128]{3,2,1,0:T(8,128)} %copy-done.3) | copy-start | bytes 3145732
  137.1 78.5 %reduce-scatter.2.cloned.1.call-start = ((), (), s32[]{:S(2)}) async-start(), calls=%async_computation.4 | async-start | bytes 1310720 | tf_op jit(solution)/shard_map/reduce_scatter | solution.py:175
  151.7 4.5 %copy-start.15 = (f32[4,8,64,128]{3,2,1,0:T(8,128)S(1)}, f32[4,8,64,128]{3,2,1,0:T(8,128)}, u32[]{:S(2)}) copy-start(f32[4,8,64,128]{3,2,1,0:T(8,128)} %convolution_subtract_fusion.6) | copy-start | bytes 3145732
  159.4 3.5 %copy-start.16 = (bf16[256,512]{1,0:T(8,128)(2,1)S(1)}, bf16[256,512]{1,0:T(8,128)(2,1)}, u32[]{:S(2)}) copy-start(bf16[256,512]{1,0:T(8,128)(2,1)} %param.22) | copy-start | bytes 786436
  159.4 3.5 %copy-start.23 = (f32[512]{0:T(512)S(1)}, f32[512]{0:T(512)}, u32[]{:S(2)}) copy-start(f32[512]{0:T(512)} %param.27) | copy-start | bytes 6148
  166.2 23.3 %copy-start.24 = (f32[128,4]{0,1:T(4,128)S(1)}, f32[128,4]{0,1:T(4,128)}, u32[]{:S(2)}) copy-start(f32[128,4]{0,1:T(4,128)} %param.32) | copy-start | bytes 6148
  166.2 23.5 %copy-start.21 = (s32[128,4]{0,1:T(4,128)S(1)}, s32[128,4]{0,1:T(4,128)}, u32[]{:S(2)}) copy-start(s32[128,4]{0,1:T(4,128)} %param.31) | copy-start | bytes 6148
  184.8 25.5 %all-to-all-start.1 = ((bf16[8,96,512]{2,1,0:T(8,128)(2,1)}), bf16[8,96,512]{2,1,0:T(8,128)(2,1)S(1)}, u32[]{:S(2)}, u32[]{:S(2)}) async-start(bf16[8,96,512]{2,1,0:T(8,128)(2,1)} %bitcast.186), calls=%async_computation.2 | async-start | bytes 1572864 | tf_op jit(solution)/shard_map/all_to_all | solution.py:257
  (10 other events, 16.6 us)
Sparse Core Ops, SparseCore 0:
  79.7 42.6 all-gather.4
  124.6 22.2 all-gather.8
  148.7 32.4 all-gather.6
  184.5 27.9 reduce-scatter.1
where the time goes:
time: 223 us; the launch traced here: 222 us
  waiting for transfers between devices  88.7 us (40%)
  matrix products  53.8 us (24%)
  local copies, waits for them, and re-layouts  37.2 us (17%)
  other arithmetic  15.9 us (7%)
  between operations  14.6 us (7%)
  starting transfers between devices  11.9 us (5%)
    dot_general x30, matrix products, product(): jnp.einsum(spec, left, right, precision=PRECISION, preferred_element_type...  32.8 us
    all_gather x1, waiting for transfers between devices, on_device(): pieces = lax.all_gather(flat_rows, 'tp', axis=1, tiled=True)  25.7 us
    all_to_all x1, waiting for transfers between devices, expert_exit(): lax.all_to_all(routed_sum.astype(jnp.bfloat16).reshape(peer_count, slot_c...  20.5 us
    all_to_all x1, waiting for transfers between devices, expert_entry(): lax.all_to_all(own_slice, 'ep', split_axis=0, concat_axis=0, tiled=True)  17.7 us
    all_gather x1, waiting for transfers between devices, expert_exit(): lax.all_gather(jnp.concatenate([routed_hidden, shared_hidden], axis=1), '...  15 us
    reshape x6, local copies, waits for them, and re-layouts, by_block(): return matrix.astype(jnp.float32).reshape(block_count, span, head_count,...  12.2 us
    all_gather x1, waiting for transfers between devices, mixer_part(): everything = lax.all_gather(whole.astype(jnp.bfloat16), 'ep')  9.73 us
    all_to_all x1, starting transfers between devices, expert_entry(): lax.all_to_all(own_slice, 'ep', split_axis=0, concat_axis=0, tiled=True)  6.49 us
  transfers between devices with their start and end apart: 6, of which 5 were waited for; matrix products, arithmetic and copies ran while one was open for 27% of the time, Pallas kernels for 0%

commit v1 on v0

--- a/solution.py
+++ b/solution.py
@@ -1,3 +1,4 @@
+import functools
 import math
 import jax
 import jax.numpy as jnp
@@ -9,6 +10,13 @@
 HIGHEST = lax.Precision.HIGHEST
 PRECISION = lax.Precision.HIGH
 NORM_FLOOR = 1.0
+
+
+def launch_sites_over_axis(field_in, mesh_ax, dim_at):
+    return jnp.concatenate(lax.all_gather(field_in, mesh_ax), dim_at)
+
+
+supply_all_values = functools.partial(launch_sites_over_axis, mesh_ax="tp", dim_at=1)
 
 
 def head_view(matrix):
@@ -306,7 +314,7 @@
         )
     )
     flat_rows = arrived.reshape(-1, arrived.shape[2])
-    pieces = lax.all_gather(flat_rows, "tp", axis=1, tiled=True)
+    pieces = supply_all_values(flat_rows)
     token_mixer_output, pieces = mixer_part(
         receptance,
         key_tensor,

time: 223 us -> 226 us (1.013)
  local copies, waits for them, and re-layouts: 37.2 us -> 41.9 us
    all_gather x0 -> x1, local copies, waits for them, and re-layouts: none -> 4.65 us  [launch_sites_over_axis(): return jnp.concatenate(lax.all_gather(field_in, mesh_ax), dim_at)]
where the time goes in v1:
time: 226 us; the launch traced here: 225 us
  waiting for transfers between devices  86.8 us (38%)
  matrix products  53.7 us (24%)
  local copies, waits for them, and re-layouts  41.9 us (19%)
  other arithmetic  15.9 us (7%)
  between operations  14.6 us (6%)
  starting transfers between devices  11.9 us (5%)
    dot_general x30, matrix products, product(): jnp.einsum(spec, left, right, precision=PRECISION, preferred_element_type...  32.8 us
    all_gather x1, waiting for transfers between devices, launch_sites_over_axis(): return jnp.concatenate(lax.all_gather(field_in, mesh_ax), dim_at)  25.8 us
    all_to_all x1, waiting for transfers between devices, expert_exit(): lax.all_to_all(routed_sum.astype(jnp.bfloat16).reshape(peer_count, slot_c...  20.5 us
    all_to_all x1, waiting for transfers between devices, expert_entry(): lax.all_to_all(own_slice, 'ep', split_axis=0, concat_axis=0, tiled=True)  17.7 us
    all_gather x1, waiting for transfers between devices, expert_exit(): lax.all_gather(jnp.concatenate([routed_hidden, shared_hidden], axis=1), '...  15 us
    reshape x6, local copies, waits for them, and re-layouts, by_block(): return matrix.astype(jnp.float32).reshape(block_count, span, head_count,...  12.2 us
    all_gather x1, waiting for transfers between devices, mixer_part(): everything = lax.all_gather(whole.astype(jnp.bfloat16), 'ep')  7.68 us
    all_to_all x1, starting transfers between devices, expert_entry(): lax.all_to_all(own_slice, 'ep', split_axis=0, concat_axis=0, tiled=True)  6.49 us
  transfers between devices with their start and end apart: 6, of which 5 were waited for; matrix products, arithmetic and copies ran while one was open for 27% of the time, Pallas kernels for 0%

profile of v1, /device:TPU:0, one launch (start us, length us, event | category | flops | bytes accessed | tf_op | source)
XLA Modules:
  0.0 224.8 jit_solution(2690978383310759128)
XLA Ops:
  10.8 2.4 %scatter_custom_fusion = s32[768]{0:T(1024)S(1)} fusion(s32[512]{0:T(512)S(1)} %bitcast.196, s32[512]{0:T(512)S(1)} %add_select_fusion, s32[]{:T(128)} %constant.328.clone.1), kind=kCustom, calls=%fused_computation.207 | custom fusion | bytes 3076 | tf_op jit(solution)/shard_map/scatter | solution.py:225
  15.9 4.3 %gather_fusion = bf16[768,2048]{1,0:T(8,128)(2,1)} fusion(bf16[129,2048]{1,0:T(8,128)(2,1)S(1)} %concatenate.33, s32[1024]{0:T(1024)S(1)} %pad_clamp_fusion.1), kind=kCustom, calls=%fused_computation | custom fusion | bytes 6294528 | tf_op jit(solution)/shard_map/jit(_take)/gather | solution.py:227
  20.2 2.3 %dynamic-slice_select_fusion = bf16[8,96,512]{2,1,0:T(8,128)(2,1)} fusion(bf16[8,96,2048]{2,1,0:T(8,128)(2,1)} %bitcast.180, s32[]{:T(128)S(6)} %select_n.364, pred[8,96]{1,0:T(8,128)(4,1)S(1)} %broadcast_in_dim.94), kind=kLoop, calls=%fused_computation.114 | loop fusion | flops 393216 | bytes 1573636 | tf_op jit(solution)/shard_map/jit(_take)/select_n | solution.py:227
  22.4 6.5 %all-to-all-start = ((bf16[8,96,512]{2,1,0:T(8,128)(2,1)}), bf16[8,96,512]{2,1,0:T(8,128)(2,1)}, u32[]{:S(2)}, u32[]{:S(2)}) async-start(bf16[8,96,512]{2,1,0:T(8,128)(2,1)} %dynamic-slice_select_fusion), calls=%async_computation | async-start | bytes 1572864 | tf_op jit(solution)/shard_map/all_to_all | solution.py:233
  29.9 2.4 %convolution_bitcast_fusion.4 = f32[256,128]{0,1:T(8,128)} fusion(bf16[128,2048]{1,0:T(8,128)(2,1)S(1)} %fusion.33, bf16[256,2048]{1,0:T(8,128)(2,1)} %param.37), kind=kOutput, calls=%fused_computation.60 | convolution fusion | flops 134217728 | bytes 1703936 | tf_op jit(solution)/shard_map/fd,rd->fr/dot_general | solution.py:195
  32.3 17.7 %all-to-all-done = bf16[8,96,512]{2,1,0:T(8,128)(2,1)} async-done(((bf16[8,96,512]{2,1,0:T(8,128)(2,1)}), bf16[8,96,512]{2,1,0:T(8,128)(2,1)}, u32[]{:S(2)}, u32[]{:S(2)}) %all-to-all-start) | async-done | bytes 786464 | tf_op jit(solution)/shard_map/all_to_all | solution.py:233
  51.0 2.1 add_divide_fusion
  57.6 2.2 reshape.837
  59.8 2.4 %reshape.888 = f32[4,64,8,64]{1,0,3,2:T(4,128)} reshape(bf16[256,512]{0,1:T(8,128)(2,1)} %copy.339) | data formatting | bytes 786432 | tf_op jit(solution)/shard_map/reshape | solution.py:104
  62.2 2.6 %copy.341 = f32[4,64,8,64]{3,1,2,0:T(8,128)} copy(f32[4,64,8,64]{1,0,3,2:T(4,128)} %reshape.888) | data formatting | bytes 1048576 | tf_op jit(solution)/shard_map/reshape | solution.py:104
  64.8 5.0 %fusion.66 = (f32[4,8,64,64]{3,2,1,0:T(8,128)S(1)}, f32[4,8,64,64]{3,2,1,0:T(8,128)S(1)}, f32[4,8,64,64]{3,2,1,0:T(8,128)S(1)}, f32[4,8,64,64]{3,2,1,0:T(8,128)S(1)}, f32[4,8,64,64]{3,2,1,0:T(8,128)}) fusion(f32[4,64,8,64]{3,2,1,0:T(8,128)} %reshape.846, f32[4,8,64]{2,1,0:T(8,128)S(1)} %add_rsqrt_fusion.1, f32[4,64,8,64]{3,1,2,0:T(8,128)S(1)} %copy.345, ...), kind=kOutput, calls=%fused_computation.113 | convolution fusion | flops 101715968 | bytes 4726784 | tf_op jit(solution)/shard_map/ts,nhsd->nhtd/dot_general | solution.py:114
  69.8 2.3 %fusion.1 = f32[4,8,128,128]{3,2,1,0:T(8,128)S(1)} fusion(f32[4,8,64,64]{3,2,1,0:T(8,128)S(1)} %get-tuple-element.30, f32[4,8,64,64]{3,2,1,0:T(8,128)S(1)} %get-tuple-element.19, f32[4,8,64,64]{3,2,1,0:T(8,128)S(1)} %get-tuple-element.18, f32[4,8,64,64]{3,2,1,0:T(8,128)S(1)} %get-tuple-element.24), kind=kOutput, calls=%fused_computation.5 | convolution fusion | flops 201850880 | bytes 4194304 | tf_op jit(solution)/shard_map/nhtd,nhsd->nhts/dot_general | solution.py:55
  79.9 2.6 %fusion.8 = f32[4,8,128,64]{3,2,1,0:T(8,128)S(1)} fusion(f32[4,8,64,64]{3,2,1,0:T(8,128)} %get-tuple-element.23, f32[4,8,64,64]{3,2,1,0:T(8,128)} %get-tuple-element.22, bf16[4,8,64,64]{3,1,2,0:T(8,128)(2,1)} %bitcast.181), kind=kOutput, calls=%fused_computation.12 | convolution fusion | flops 100925440 | bytes 2359296 | tf_op jit(solution)/shard_map/nhts,nhsd->nhtd/dot_general | solution.py:55
  96.7 25.8 %all-gather.5.cloned.1.call-done = bf16[4,768,512]{2,1,0:T(8,128)(2,1)} async-done(((bf16[1,768,512]{2,1,0:T(8,128)(2,1)}), bf16[4,768,512]{2,1,0:T(8,128)(2,1)}) %all-gather.5.cloned.1.call-update) | async-done | bytes 3145744 | tf_op jit(solution)/shard_map/all_gather | solution.py:16
  122.5 4.6 %copy.360 = bf16[4,768,512]{1,2,0:T(8,128)(2,1)} copy(bf16[4,768,512]{2,1,0:T(8,128)(2,1)} %all-gather.5.cloned.1.call-done) | data formatting | bytes 6291456 | tf_op jit(solution)/shard_map/all_gather | solution.py:16
  127.5 2.5 %fusion.30 = bf16[256,128]{0,1:T(8,128)(2,1)} fusion(bf16[128,2048]{1,0:T(8,128)(2,1)} %copy-done.14, bf16[256,2048]{1,0:T(8,128)(2,1)} %param.38, f32[256,128]{0,1:T(8,128)S(1)} %copy-done.20), kind=kOutput, calls=%fused_computation.61 | convolution fusion | flops 134414336 | bytes 1769472 | tf_op jit(solution)/shard_map/fd,rd->fr/dot_general | solution.py:196
  134.8 3.9 %convolution_subtract_fusion.6 = f32[4,8,64,128]{3,2,1,0:T(8,128)} fusion(f32[4,8,64,128]{3,2,1,0:T(8,128)} %copy-done.10, f32[4,8,128,128]{3,2,1,0:T(8,128)} %copy-done.1, f32[4,8,64,64]{3,2,1,0:T(8,128)} %get-tuple-element.20, f32[4,8,64,64]{3,2,1,0:T(8,128)S(1)} %copy-done.9, pred[64,64]{1,0:T(8,128)(4,1)S(1)} %iota_compare_fusion.2), kind=kOutput, calls=%fused_computation.27 | convolution fusion | flops 101318656 | bytes 4722688 | tf_op jit(solution)/shard_map/nhts,nhsd->nhtd/dot_general | solution.py:55
  141.9 7.7 %all-gather.9.cloned.1.call-done = bf16[64,64,128]{2,1,0:T(8,128)(2,1)} async-done(((bf16[8,64,128]{2,1,0:T(8,128)(2,1)}), bf16[64,64,128]{2,1,0:T(8,128)(2,1)}) %all-gather.9.cloned.1.call-update) | async-done | bytes 1048592 | tf_op jit(solution)/shard_map/all_gather | solution.py:154
  165.6 3.2 %convolution_convert_fusion = bf16[256,2048]{1,0:T(8,128)(2,1)} fusion(bf16[512,2048]{1,0:T(8,128)(2,1)S(1)} %copy-done, bf16[256,512]{1,0:T(8,128)(2,1)} %param.25, f32[256,512]{1,0:T(8,128)} %copy.368, bf16[256,512]{1,0:T(8,128)(2,1)S(1)} %copy-done.17, f32[256,512]{1,0:T(8,128)} %copy.367, f32[256,512]{1,0:T(8,128)} %reshape.842, ...), kind=kOutput, calls=%fused_computation.4 | convolution fusion | flops 538574848 | bytes 5769216 | tf_op jit(solution)/shard_map/dot_general | solution.py:184
  168.9 15.0 %all-gather.7.cloned.1.call-done = bf16[1024,896]{0,1:T(8,128)(2,1)} async-done(((bf16[256,896]{0,1:T(8,128)(2,1)}), bf16[1024,896]{0,1:T(8,128)(2,1)}) %all-gather.7.cloned.1.call-update) | async-done | bytes 1835024 | tf_op jit(solution)/shard_map/all_gather | solution.py:256
  183.9 3.6 %fusion.14 = bf16[768,512]{1,0:T(8,128)(2,1)} fusion(bf16[1024,896]{0,1:T(8,128)(2,1)} %all-gather.7.cloned.1.call-done, bf16[1,1024,512]{2,1,0:T(8,128)(2,1)} %param.36), kind=kOutput, calls=%fused_computation.23 | convolution fusion | flops 805699584 | bytes 3407872 | tf_op jit(solution)/shard_map/fr,fd->rd/dot_general | solution.py:261
  187.4 4.6 %all-to-all-start.1 = ((bf16[8,96,512]{2,1,0:T(8,128)(2,1)}), bf16[8,96,512]{2,1,0:T(8,128)(2,1)S(1)}, u32[]{:S(2)}, u32[]{:S(2)}) async-start(bf16[8,96,512]{2,1,0:T(8,128)(2,1)} %bitcast.191), calls=%async_computation.2 | async-start | bytes 1572864 | tf_op jit(solution)/shard_map/all_to_all | solution.py:265
  192.5 20.5 %all-to-all-done.1 = bf16[8,96,512]{2,1,0:T(8,128)(2,1)S(1)} async-done(((bf16[8,96,512]{2,1,0:T(8,128)(2,1)}), bf16[8,96,512]{2,1,0:T(8,128)(2,1)S(1)}, u32[]{:S(2)}, u32[]{:S(2)}) %all-to-all-start.1) | async-done | bytes 786464 | tf_op jit(solution)/shard_map/all_to_all | solution.py:265
  216.0 2.3 %fusion.28 = bf16[128,512]{1,0:T(8,128)(2,1)} fusion(f32[128,512]{1,0:T(8,128)S(1)} %multiply_reduce_fusion, bf16[1024,512]{1,0:T(8,128)(2,1)} %param.39, bf16[1024,896]{0,1:T(8,128)(2,1)} %all-gather.7.cloned.1.call-done), kind=kOutput, calls=%fused_computation.57 | convolution fusion | flops 134348800 | bytes 1703936 | tf_op jit(solution)/shard_map/fr,fd->rd/dot_general | solution.py:262
  (176 shorter events, 61.7 us)
Async XLA Ops:
  7.2 158.4 %copy-start = (bf16[512,2048]{1,0:T(8,128)(2,1)S(1)}, bf16[512,2048]{1,0:T(8,128)(2,1)}, u32[]{:S(2)}) copy-start(bf16[512,2048]{1,0:T(8,128)(2,1)} %param.29) | copy-start | bytes 6291460
  15.8 14.1 %copy-start.14 = (bf16[128,2048]{1,0:T(8,128)(2,1)}, bf16[128,2048]{1,0:T(8,128)(2,1)S(1)}, u32[]{:S(2)}) copy-start(bf16[128,2048]{1,0:T(8,128)(2,1)S(1)} %fusion.33) | copy-start | bytes 1572868
  22.4 27.5 %copy-start.18 = (bf16[256,512]{1,0:T(8,128)(2,1)S(1)}, bf16[256,512]{1,0:T(8,128)(2,1)}, u32[]{:S(2)}) copy-start(bf16[256,512]{1,0:T(8,128)(2,1)} %param.21) | copy-start | bytes 786436
  22.4 27.7 %copy-start.19 = (bf16[256,512]{1,0:T(8,128)(2,1)S(1)}, bf16[256,512]{1,0:T(8,128)(2,1)}, u32[]{:S(2)}) copy-start(bf16[256,512]{1,0:T(8,128)(2,1)} %param.20) | copy-start | bytes 786436
  22.4 28.5 %copy-start.23 = (f32[512]{0:T(512)S(1)}, f32[512]{0:T(512)}, u32[]{:S(2)}) copy-start(f32[512]{0:T(512)} %param.26) | copy-start | bytes 6148
  22.4 27.5 %all-to-all-start = ((bf16[8,96,512]{2,1,0:T(8,128)(2,1)}), bf16[8,96,512]{2,1,0:T(8,128)(2,1)}, u32[]{:S(2)}, u32[]{:S(2)}) async-start(bf16[8,96,512]{2,1,0:T(8,128)(2,1)} %dynamic-slice_select_fusion), calls=%async_computation | async-start | bytes 1572864 | tf_op jit(solution)/shard_map/all_to_all | solution.py:233
  28.9 93.6 %all-gather.5.cloned.1.call-start = ((), (), s32[]{:S(2)}) async-start(), calls=%async_computation.3 | async-start | bytes 3932160 | tf_op jit(solution)/shard_map/all_gather | solution.py:16
  72.1 2.8 %copy-start.1 = (f32[4,8,128,128]{3,2,1,0:T(8,128)}, f32[4,8,128,128]{3,2,1,0:T(8,128)S(1)}, u32[]{:S(2)}) copy-start(f32[4,8,128,128]{3,2,1,0:T(8,128)S(1)} %fusion.1) | copy-start | bytes 6291460
  79.6 70.0 %all-gather.9.cloned.1.call-start = ((), (), s32[]{:S(2)}) async-start(), calls=%async_computation.6 | async-start | bytes 1179648 | tf_op jit(solution)/shard_map/all_gather | solution.py:154
  79.8 2.8 %copy-start.2 = (f32[4,8,128,128]{3,2,1,0:T(8,128)S(1)}, f32[4,8,128,128]{3,2,1,0:T(8,128)}, u32[]{:S(2)}) copy-start(f32[4,8,128,128]{3,2,1,0:T(8,128)} %copy-done.1) | copy-start | bytes 6291460
  91.2 3.5 %copy-start.10 = (f32[4,8,64,128]{3,2,1,0:T(8,128)}, f32[4,8,64,128]{3,2,1,0:T(8,128)S(1)}, u32[]{:S(2)}) copy-start(f32[4,8,64,128]{3,2,1,0:T(8,128)S(1)} %fusion.35) | copy-start | bytes 3145732
  96.7 30.8 %copy-start.20 = (f32[256,128]{0,1:T(8,128)S(1)}, f32[256,128]{0,1:T(8,128)}, u32[]{:S(2)}) copy-start(f32[256,128]{0,1:T(8,128)} %convolution_bitcast_fusion.4) | copy-start | bytes 393220
  127.2 7.6 %copy-start.9 = (f32[4,8,64,64]{3,2,1,0:T(8,128)S(1)}, f32[4,8,64,64]{3,2,1,0:T(8,128)}, u32[]{:S(2)}) copy-start(f32[4,8,64,64]{3,2,1,0:T(8,128)} %copy-done.8) | copy-start | bytes 1572868
  127.2 56.7 %all-gather.7.cloned.1.call-start = ((), (), s32[]{:S(2)}) async-start(), calls=%async_computation.5 | async-start | bytes 2293760 | tf_op jit(solution)/shard_map/all_gather | solution.py:256
  134.8 3.9 %copy-start.16 = (bf16[4,768,512]{1,2,0:T(8,128)(2,1)S(1)}, bf16[4,768,512]{1,2,0:T(8,128)(2,1)}, u32[]{:S(2)}) copy-start(bf16[4,768,512]{1,2,0:T(8,128)(2,1)} %copy.360) | copy-start | bytes 9437188
  134.8 3.9 %copy-start.26 = (bf16[1,256,2048]{2,1,0:T(8,128)(2,1)S(1)}, bf16[1,256,2048]{2,1,0:T(8,128)(2,1)}, u32[]{:S(2)}) copy-start(bf16[1,256,2048]{2,1,0:T(8,128)(2,1)} %param.34) | copy-start | bytes 3145732
  141.8 16.3 %copy-start.4 = (f32[4,8,64,128]{3,2,1,0:T(8,128)S(1)}, f32[4,8,64,128]{3,2,1,0:T(8,128)}, u32[]{:S(2)}) copy-start(f32[4,8,64,128]{3,2,1,0:T(8,128)} %copy-done.3) | copy-start | bytes 3145732
  141.8 76.4 %reduce-scatter.2.cloned.1.call-start = ((), (), s32[]{:S(2)}) async-start(), calls=%async_computation.4 | async-start | bytes 1310720 | tf_op jit(solution)/shard_map/reduce_scatter | solution.py:183
  154.4 4.5 %copy-start.15 = (f32[4,8,64,128]{3,2,1,0:T(8,128)S(1)}, f32[4,8,64,128]{3,2,1,0:T(8,128)}, u32[]{:S(2)}) copy-start(f32[4,8,64,128]{3,2,1,0:T(8,128)} %convolution_subtract_fusion.6) | copy-start | bytes 3145732
  162.1 3.5 %copy-start.17 = (bf16[256,512]{1,0:T(8,128)(2,1)S(1)}, bf16[256,512]{1,0:T(8,128)(2,1)}, u32[]{:S(2)}) copy-start(bf16[256,512]{1,0:T(8,128)(2,1)} %param.22) | copy-start | bytes 786436
  162.1 3.5 %copy-start.24 = (f32[512]{0:T(512)S(1)}, f32[512]{0:T(512)}, u32[]{:S(2)}) copy-start(f32[512]{0:T(512)} %param.27) | copy-start | bytes 6148
  168.8 23.3 %copy-start.25 = (f32[128,4]{0,1:T(4,128)S(1)}, f32[128,4]{0,1:T(4,128)}, u32[]{:S(2)}) copy-start(f32[128,4]{0,1:T(4,128)} %param.32) | copy-start | bytes 6148
  168.9 23.5 %copy-start.22 = (s32[128,4]{0,1:T(4,128)S(1)}, s32[128,4]{0,1:T(4,128)}, u32[]{:S(2)}) copy-start(s32[128,4]{0,1:T(4,128)} %param.31) | copy-start | bytes 6148
  187.4 25.5 %all-to-all-start.1 = ((bf16[8,96,512]{2,1,0:T(8,128)(2,1)}), bf16[8,96,512]{2,1,0:T(8,128)(2,1)S(1)}, u32[]{:S(2)}, u32[]{:S(2)}) async-start(bf16[8,96,512]{2,1,0:T(8,128)(2,1)} %bitcast.191), calls=%async_computation.2 | async-start | bytes 1572864 | tf_op jit(solution)/shard_map/all_to_all | solution.py:265
  (10 other events, 16.6 us)
Sparse Core Ops, SparseCore 0:
  79.7 42.7 all-gather.4
  127.3 22.2 all-gather.8
  151.4 32.4 all-gather.6
  187.2 27.9 reduce-scatter.1
